TPU v7x, 32 devices: a whole 2x2x4 slice. The times are simulated.
32 devices in a mesh: sp: 8 (over z, x), tp: 4 (over y, core).
Axes of the slice: x: 2, y: 2, z: 4, core: 2. Of those that a mesh axis runs over, the one named last changes fastest.
Arguments:
- result_cotangent_values: bfloat16 [1024, 2048], P('sp'), may hold values from -6 to 6
- specialist_entry_vectors: bfloat16 [1024, 2048], P('sp'), may hold values from -6 to 6
- chosen_specialists: int32 [1024, 2], P('sp'), may hold values from 0 to 3, all different within a row; in each aligned block of 128 rows (0 to 127, 128 to 255, ...) at most 128 rows name the same one
- specialist_mixing_shares: float32 [1024, 2], P('sp'), may hold values from 0.1 to 0.9
- specialist_switch_maps: bfloat16 [8, 2048, 1792], P('sp', None, 'tp'), may hold values from -0.125 to 0.125
- specialist_widen_maps: bfloat16 [8, 2048, 1792], P('sp', None, 'tp'), may hold values from -0.125 to 0.125
- specialist_shrink_maps: bfloat16 [8, 1792, 2048], P('sp', 'tp'), may hold values from -0.09375 to 0.09375
- memory_readout_map: bfloat16 [2048, 2048], P('sp', 'tp'), may hold values from -0.125 to 0.125
- memory_source_vectors: bfloat16 [1024, 2048], P('sp', 'tp'), may hold values from -6 to 6
- memory_hidden_values: bfloat16 [1024, 2048], P('sp', 'tp'), may hold values from -6 to 6
- feature_fading_speed: float32 [2048], P('tp'), may hold values from 1.6276042e-05 to 0.009
- extra_log_fading: float32 [1024], P('sp'), may hold values from -2.8 to 0
- memory_switch_tiles: bfloat16 [8, 256, 256], P('tp'), may hold values from -0.375 to 0.375
- entry_switch_tiles: bfloat16 [8, 256, 256], P('tp'), may hold values from -0.375 to 0.375
Outputs:
- gate_proj_grad: bfloat16 [8, 2048, 1792], P('sp', None, 'tp')
- up_proj_grad: bfloat16 [8, 2048, 1792], P('sp', None, 'tp')
- down_proj_grad: bfloat16 [8, 1792, 2048], P('sp', 'tp')
- out_proj_grad: float32 [2048, 2048], P('sp', 'tp')
- lru_input_grad: float32 [1024, 2048], P('sp', 'tp')
Inputs may be any that keep to these rules, and one draw needn't show every extreme that they name: `chosen_specialists`: each token names two different experts; among the 128 tokens of one device no expert is named more than 128 times, a bound that some block reaches on some device.
All inputs are finite; a program needn't handle non-finite values.
Results may differ from a plain program's by a relative error of at most 0.009.
Values may be sent and summed in bfloat16 or wider, within the bound.
A program may use at most 128 MiB of HBM per device.

v0:
```python
import functools

import jax
import jax.numpy as jnp
from jax import lax
from jax.experimental import pallas as pl
from jax.experimental.pallas import tpu as pltpu
from jax.sharding import PartitionSpec as P

SLICES = 2


def prefix(part, axis, combine, identity):
    count = lax.axis_size(axis)
    place = lax.axis_index(axis)
    ahead = count - 1 - place
    gathered = jax.tree.map(lambda a: lax.all_gather(a, axis), part)
    state = jax.tree.map(lambda a, e: jnp.zeros_like(a) + jnp.asarray(e, a.dtype), part, identity)

    def one(turn, state):
        source = count - 1 - turn
        return combine(
            state, jax.tree.map(lambda a: lax.dynamic_index_in_dim(a, source, 0, False), gathered)
        )

    return lax.fori_loop(0, ahead, one, state)


def silu_slope(value):
    sig_value = jax.nn.sigmoid(value)
    return sig_value * (1.0 + value * (1.0 - sig_value))


def compose(upper_map, lower_map):
    return (lower_map[0] * upper_map[0], lower_map[1] + lower_map[0] * upper_map[1])


def chain_join(higher_map, lower_map):
    return (lower_map[0] * higher_map[0], lower_map[1] + lower_map[0] * higher_map[1])


def expert_backward(inputs, grads_in, gate_weight, up_weight, down_weight):
    gate_value = jnp.dot(inputs, gate_weight, preferred_element_type=jnp.float32)
    up_value = jnp.dot(inputs, up_weight, preferred_element_type=jnp.float32)
    active = jax.nn.silu(gate_value)
    hidden = (active * up_value).astype(jnp.bfloat16)
    down_grad = jnp.einsum(
        "rf,rd->fd", hidden, grads_in, preferred_element_type=jnp.float32
    ).astype(jnp.bfloat16)
    hidden_grad = jnp.einsum("rd,fd->rf", grads_in, down_weight, preferred_element_type=jnp.float32)
    gate_grad = (hidden_grad * up_value * silu_slope(gate_value)).astype(jnp.bfloat16)
    up_grad = (hidden_grad * active).astype(jnp.bfloat16)
    gate_weight_grad = jnp.einsum(
        "rd,rf->df", inputs, gate_grad, preferred_element_type=jnp.float32
    ).astype(jnp.bfloat16)
    up_weight_grad = jnp.einsum(
        "rd,rf->df", inputs, up_grad, preferred_element_type=jnp.float32
    ).astype(jnp.bfloat16)
    token_part = jnp.einsum("rf,df->rd", gate_grad, gate_weight, preferred_element_type=jnp.float32)
    token_part = token_part + jnp.einsum(
        "rf,df->rd", up_grad, up_weight, preferred_element_type=jnp.float32
    )
    return (gate_weight_grad, up_weight_grad, down_grad, token_part)


def collect(returned, targets, route_count):
    gathered = jnp.take(returned, targets[0], axis=0).astype(jnp.float32)
    for target in targets[1:]:
        gathered = gathered + jnp.take(returned, target, axis=0).astype(jnp.float32)
    return gathered.reshape(-1, route_count, gathered.shape[-1]).sum(axis=1)


def fill_slots(values, targets, slot_rows):
    buffer = jnp.zeros((slot_rows, values.shape[1]), jnp.bfloat16)
    for target in targets:
        buffer = buffer.at[target].set(values)
    return buffer


MESH_ID = pl.DeviceIdType.MESH


def greet(peers):
    barrier = pltpu.get_barrier_semaphore()
    for peer in peers:
        pl.semaphore_signal(barrier, inc=1, device_id=peer, device_id_type=MESH_ID)
    pl.semaphore_wait(barrier, len(peers))


def remote(src, dst, send, recv, peer):
    return pltpu.make_async_remote_copy(
        src_ref=src, dst_ref=dst, send_sem=send, recv_sem=recv, device_id=peer, device_id_type=MESH_ID
    )


def places(sp_count):
    me = lax.axis_index("sp")
    tp = lax.axis_index("tp")
    side, core = tp // 2, tp % 2
    peers = [(lax.rem(me + k, sp_count), tp) for k in range(sp_count)]
    sources = [lax.rem(me + sp_count - k, sp_count) for k in range(sp_count)]
    sibling = (me, side * 2 + (1 - core))
    across = (me, (1 - side) * 2 + core)
    return me, side, core, peers, sources, sibling, across


def gather_kernel(sp_count, x_ref, g_ref, info_ref, r_ref, h_ref, xo, go, io, ro, ho,
                  zs, zr, xs, xr, ys, yr, ss, sr, ts, tr, local_sem):
    me, side, core, peers, sources, sibling, across = places(sp_count)
    tp = lax.axis_index("tp")
    rows, feats = x_ref.shape
    half = feats // 2
    passed = 3 * half // 8
    direct = half - passed
    first = pl.multiple_of(core * half + side * passed, 128)
    onward = pl.multiple_of(core * half + side * direct, 128)
    back = pl.multiple_of(core * half + (1 - side) * direct, 128)
    depth = sp_count // 2
    z, x = me // 2, me % 2
    partner = (z * 2 + 1 - x, tp)
    along = [(lax.rem(z + k, depth) * 2 + x, tp) for k in range(depth)]
    line = [lax.rem(z + depth - k, depth) * 2 for k in range(depth)]

    def at(ref, who, col, width):
        return ref.at[pl.ds(pl.multiple_of(who * rows, rows), rows), pl.ds(col, width)]

    def block(ref, who, size):
        return ref.at[pl.ds(pl.multiple_of(who * size, size), size), :]

    greet(along[1:] + [partner, sibling, across])
    pairs = ((x_ref, xo), (g_ref, go))
    small = ((info_ref, io), (r_ref, ro), (h_ref, ho))
    waits = []
    recv = {}

    def send(key, src, dst, sems, index, peer):
        cp = remote(src, dst, sems[0].at[index], sems[1].at[index], peer)
        cp.start()
        recv[key] = cp

    for n, (src, dst) in enumerate(pairs + small):
        cp = pltpu.make_async_copy(src, block(dst, me, src.shape[0]), local_sem.at[n])
        cp.start()
        waits.append(cp)

    def open_pair(a):
        src, dst = pairs[a]
        for k in range(depth - 1, 0, -1):
            send(("z", a, k), src.at[:, pl.ds(first, direct)], at(dst, me, first, direct), (zs, zr), (a, k), along[k])
        send(("x", a, 0), src.at[:, pl.ds(first, direct)], at(dst, me, first, direct), (xs, xr), (a, 0), partner)

    def spread(a, who, n):
        dst = pairs[a][1]
        send(("y", a, n), at(dst, who, onward, passed), at(dst, who, onward, passed), (ys, yr), (a, n), across)
        send(("s", a, n), at(dst, who, first, direct), at(dst, who, first, direct), (ss, sr), (a, n), sibling)

    def open_small(b):
        src, dst = small[b]
        size = src.shape[0]
        for k in range(depth - 1, 0, -1):
            send(("z", 2 + b, k), src, block(dst, me, size), (zs, zr), (2 + b, k), along[k])
        send(("x", 2 + b, 0), src, block(dst, me, size), (xs, xr), (2 + b, 0), partner)

    open_pair(0)
    open_small(0)
    open_pair(1)
    for a in range(2):
        for k in range(1, depth):
            recv["z", a, k].wait_recv()
            who = line[k] + x
            dst = pairs[a][1]
            send(("x", a, k), at(dst, who, first, direct), at(dst, who, first, direct), (xs, xr), (a, k), partner)
            spread(a, who, k)
        if a == 1:
            open_small(1)
            open_small(2)
        for k in range(depth):
            recv["x", a, k].wait_recv()
            spread(a, line[k] + 1 - x, depth + k)
    for b in range(3):
        dst = small[b][1]
        size = small[b][0].shape[0]
        for k in range(1, depth):
            recv["z", 2 + b, k].wait_recv()
            who = line[k] + x
            send(("x", 2 + b, k), block(dst, who, size), block(dst, who, size), (xs, xr), (2 + b, k), partner)
    for a in range(2):
        dst = pairs[a][1]
        for n in range(1, 2 * depth):
            recv["y", a, n].wait_recv()
            who = line[n] + x if n < depth else line[n - depth] + 1 - x
            send(("t", a, n), at(dst, who, back, passed), at(dst, who, back, passed), (ts, tr), (a, n), sibling)
    for b in range(3):
        for k in range(depth):
            recv["x", 2 + b, k].wait_recv()
    for a in range(2):
        for n in range(1, 2 * depth):
            recv["s", a, n].wait_recv()
            recv["t", a, n].wait_recv()
    for cp in recv.values():
        cp.wait_send()
    for cp in waits:
        cp.wait()


def gather_all(sp_count, x, g, info, r, h):
    dma = pltpu.SemaphoreType.DMA
    outs = [jax.ShapeDtypeStruct((a.shape[0] * sp_count, a.shape[1]), a.dtype) for a in (x, g, info, r, h)]
    return pl.pallas_call(
        functools.partial(gather_kernel, sp_count),
        out_shape=outs,
        in_specs=[pl.BlockSpec(memory_space=pltpu.VMEM)] * 5,
        out_specs=[pl.BlockSpec(memory_space=pl.ANY)] * 5,
        scratch_shapes=[dma((5, sp_count))] * 4 + [dma((2, sp_count))] * 6 + [dma((5,))],
        compiler_params=pltpu.CompilerParams(collective_id=0, has_side_effects=True),
    )(x, g, info, r, h)


def return_kernel(sp_count, p_ref, g_ref, mixed, sib, out, ygot, last, got,
                  a_s, a_r, y_s, y_r, b_s, b_r, c_s, c_r):
    me, side, core, peers, sources, sibling, across = places(sp_count)
    rows, feats = g_ref.shape
    half, quarter = feats // 2, feats // 4
    mine = pl.multiple_of(core * half, half)
    theirs = pl.multiple_of((1 - core) * half, half)
    own = pl.ds(pl.multiple_of(side * quarter, quarter), quarter)
    other = pl.ds(pl.multiple_of((1 - side) * quarter, quarter), quarter)
    greet(peers[1:] + [sibling, across])
    order = list(range(sp_count // 2, 0, -1)) + list(range(sp_count // 2 + 1, sp_count)) + [0]
    first, second, third = {}, {}, {}
    for k in order:
        at = pl.ds(pl.multiple_of(peers[k][0] * rows, rows), rows)
        first[k] = remote(p_ref.at[at, pl.ds(theirs, half)], sib.at[k], a_s.at[k], a_r.at[k], sibling)
        first[k].start()
    for k in order:
        at = pl.ds(pl.multiple_of(peers[k][0] * rows, rows), rows)
        first[k].wait_recv()
        total = p_ref[at, pl.ds(mine, half)].astype(jnp.float32) + sib[k].astype(jnp.float32)
        out[k] = total.astype(jnp.bfloat16)
        second[k] = remote(out.at[k, :, other], ygot.at[k], y_s.at[k], y_r.at[k], across)
        second[k].start()
    for k in order:
        second[k].wait_recv()
        total = out[k, :, own].astype(jnp.float32) + ygot[k].astype(jnp.float32)
        last[k] = total.astype(jnp.bfloat16)
        if k:
            third[k] = remote(last.at[k], got.at[k], b_s.at[k], b_r.at[k], peers[k])
            third[k].start()
    total = last[0].astype(jnp.float32)
    for k in order[:-1]:
        third[k].wait_recv()
        total = total + got[k].astype(jnp.float32)
    here = pl.ds(pl.multiple_of(core * half + side * quarter, quarter), quarter)
    there = pl.ds(pl.multiple_of(core * half + (1 - side) * quarter, quarter), quarter)
    mixed[:, here] = (g_ref[:, here].astype(jnp.float32) + total).astype(jnp.bfloat16)
    ends = []
    for n, (cols, who) in enumerate(((here, across), (here, sibling), (there, sibling))):
        if n == 2:
            ends[0].wait_recv()
        cp = remote(mixed.at[:, cols], mixed.at[:, cols], c_s.at[n], c_r.at[n], who)
        cp.start()
        ends.append(cp)
    ends[1].wait_recv()
    ends[2].wait_recv()
    for cp in ends + list(first.values()) + list(second.values()) + list(third.values()):
        cp.wait_send()


def return_all(sp_count, partial, g):
    dma = pltpu.SemaphoreType.DMA
    rows, feats = g.shape
    big = pltpu.VMEM((sp_count, rows, feats // 2), jnp.bfloat16)
    small = pltpu.VMEM((sp_count, rows, feats // 4), jnp.bfloat16)
    return pl.pallas_call(
        functools.partial(return_kernel, sp_count),
        out_shape=jax.ShapeDtypeStruct((rows, feats), jnp.bfloat16),
        in_specs=[pl.BlockSpec(memory_space=pltpu.VMEM)] * 2,
        out_specs=pl.BlockSpec(memory_space=pltpu.VMEM),
        scratch_shapes=[big, big, small, small, small] + [dma((sp_count,))] * 6 + [dma((3,))] * 2,
        compiler_params=pltpu.CompilerParams(collective_id=1, has_side_effects=True),
    )(partial, g)


def carry_kernel(sp_count, mixed, decay_ref, up_ref, dstate, cols_out, block, got, s, r, d_s, d_r, local_sem):
    me, side, core, peers, sources, sibling, across = places(sp_count)
    rows, feats = mixed.shape
    width = feats // sp_count
    greet(peers[1:])
    own = pl.ds(pl.multiple_of(me * rows, rows), rows)
    moved = []
    for k in range(1, sp_count):
        cols = pl.ds(pl.multiple_of(peers[k][0] * width, width), width)
        cp = remote(mixed.at[:, cols], cols_out.at[own, :], d_s.at[k], d_r.at[k], peers[k])
        cp.start()
        moved.append(cp)
    here = pltpu.make_async_copy(
        mixed.at[:, pl.ds(pl.multiple_of(me * width, width), width)], cols_out.at[own, :], local_sem
    )
    here.start()
    row = lax.broadcasted_iota(jnp.int32, up_ref.shape, 0)
    decay = decay_ref[...]
    prod = jnp.where(row < rows - 1, pltpu.roll(decay, rows - 1, 0), 1.0)
    part = up_ref[...]
    step = 1
    while step < rows:
        keep = row < rows - step
        later = jnp.where(keep, pltpu.roll(part, rows - step, 0), 0.0)
        after = jnp.where(keep, pltpu.roll(prod, rows - step, 0), 1.0)
        part = part + prod * later
        prod = prod * after
        step *= 2
    block[...] = jnp.zeros_like(block)
    got[me] = jnp.zeros(block.shape, jnp.float32)
    block[0:1] = decay[0:1] * prod[0:1]
    block[1:2] = decay[0:1] * part[0:1]
    copies = []
    for k in range(1, sp_count):
        cp = remote(block, got.at[me], s.at[k], r.at[k], peers[k])
        cp.start()
        copies.append(cp)
    for cp in copies:
        cp.wait()
    incoming = jnp.zeros((1, up_ref.shape[1]), jnp.float32)
    for source in range(sp_count - 1, 0, -1):
        value = got[source]
        incoming = jnp.where(source > me, value[1:2] + value[0:1] * incoming, incoming)
    dstate[...] = part + prod * incoming
    here.wait()
    for cp in moved:
        cp.wait()


def carry_all(sp_count, mixed, decay, upstream):
    dma = pltpu.SemaphoreType.DMA
    rows, feats = mixed.shape
    block = (8, upstream.shape[1])
    return pl.pallas_call(
        functools.partial(carry_kernel, sp_count),
        out_shape=[
            jax.ShapeDtypeStruct(upstream.shape, jnp.float32),
            jax.ShapeDtypeStruct((rows * sp_count, feats // sp_count), jnp.bfloat16),
        ],
        in_specs=[pl.BlockSpec(memory_space=pltpu.VMEM)] * 3,
        out_specs=[pl.BlockSpec(memory_space=pltpu.VMEM)] * 2,
        scratch_shapes=[pltpu.VMEM(block, jnp.float32), pltpu.VMEM((sp_count,) + block, jnp.float32)]
        + [dma((sp_count,))] * 4
        + [dma],
        compiler_params=pltpu.CompilerParams(collective_id=2, has_side_effects=True),
    )(mixed, decay, upstream)


def local(
    result_cotangent_values,
    specialist_entry_vectors,
    chosen_specialists,
    specialist_mixing_shares,
    specialist_switch_maps,
    specialist_widen_maps,
    specialist_shrink_maps,
    memory_readout_map,
    memory_source_vectors,
    memory_hidden_values,
    feature_fading_speed,
    extra_log_fading,
    memory_switch_tiles,
    entry_switch_tiles,
):
    tok_rows, feature_count = result_cotangent_values.shape
    route_count = chosen_specialists.shape[1]
    sp_count = lax.axis_size("sp")
    expert_count = sp_count // SLICES
    capacity = min(tok_rows, 4 * tok_rows // expert_count)
    slot_rows = sp_count * capacity
    flat_expert = chosen_specialists.reshape(-1)
    onehot = (flat_expert[:, None] == jnp.arange(expert_count, dtype=jnp.int32)[None, :]).astype(
        jnp.int32
    )
    slot_rank = jnp.sum((jnp.cumsum(onehot, axis=0) - 1) * onehot, axis=1)
    scaled = (
        (
            specialist_mixing_shares[:, :, None]
            * result_cotangent_values[:, None, :].astype(jnp.float32)
        )
        .astype(jnp.bfloat16)
        .reshape(-1, feature_count)
    )
    copies = jnp.broadcast_to(
        specialist_entry_vectors[:, None, :], (tok_rows, route_count, feature_count)
    ).reshape(-1, feature_count)
    targets = [
        (flat_expert * SLICES + slice_index) * capacity + slot_rank for slice_index in range(SLICES)
    ]
    share = feature_count // lax.axis_size("tp")
    first_col = lax.axis_index("tp") * share
    part_grad = lax.dynamic_slice_in_dim(scaled, first_col, share, 1)
    part_rows = lax.dynamic_slice_in_dim(copies, first_col, share, 1)
    send_grad = fill_slots(part_grad, targets, slot_rows)
    send_rows = fill_slots(part_rows, targets, slot_rows)
    got_grad, got_rows = (
        lax.all_to_all(
            send_grad.reshape(sp_count, capacity, share),
            "sp",
            split_axis=0,
            concat_axis=0,
            tiled=True,
        ),
        lax.all_to_all(
            send_rows.reshape(sp_count, capacity, share),
            "sp",
            split_axis=0,
            concat_axis=0,
            tiled=True,
        ),
    )
    recv_grad, recv_rows = (
        lax.all_gather(got_grad, "tp", axis=2, tiled=True),
        lax.all_gather(got_rows, "tp", axis=2, tiled=True),
    )
    inputs = recv_rows.reshape(slot_rows, feature_count)
    grads_in = recv_grad.reshape(slot_rows, feature_count)
    gate_weight_grad, up_weight_grad, down_grad, token_part = expert_backward(
        inputs,
        grads_in,
        specialist_switch_maps[0],
        specialist_widen_maps[0],
        specialist_shrink_maps[0],
    )
    returned = lax.all_to_all(
        token_part.astype(jnp.bfloat16).reshape(sp_count, capacity, feature_count),
        "sp",
        split_axis=0,
        concat_axis=0,
        tiled=True,
    )
    own_sum = collect(returned.reshape(slot_rows, feature_count), targets, route_count)
    moe_grad = lax.psum(own_sum.astype(jnp.bfloat16), "tp").astype(jnp.float32)
    mixed_grad = (result_cotangent_values.astype(jnp.float32) + moe_grad).astype(jnp.bfloat16)
    col_count = memory_readout_map.shape[1]
    columns = mixed_grad
    upstream = jnp.dot(
        columns,
        lax.all_gather(memory_readout_map, "sp", axis=0, tiled=True),
        preferred_element_type=jnp.float32,
    )
    blocks_here = memory_switch_tiles.shape[0]
    block_width = memory_switch_tiles.shape[1]
    blocks_in = memory_source_vectors.reshape(tok_rows, blocks_here, block_width)
    memory_switch_fraction = jax.nn.sigmoid(
        jnp.einsum(
            "tnc,ncd->tnd", blocks_in, memory_switch_tiles, preferred_element_type=jnp.float32
        ).reshape(tok_rows, col_count)
    )
    inp_open = jax.nn.sigmoid(
        jnp.einsum(
            "tnc,ncd->tnd", blocks_in, entry_switch_tiles, preferred_element_type=jnp.float32
        ).reshape(tok_rows, col_count)
    )
    xin = memory_source_vectors.astype(jnp.float32)
    log_fading_factor = (
        -8.0 * memory_switch_fraction * feature_fading_speed[None, :] + extra_log_fading[:, None]
    )
    decay_mult = jnp.exp(log_fading_factor)
    spare_room = -jnp.expm1(2.0 * log_fading_factor)
    in_scale = jnp.sqrt(jnp.maximum(spare_room, 0.01))
    drive = in_scale * inp_open * xin
    coeff = jnp.concatenate([decay_mult[1:], jnp.ones((1, col_count), jnp.float32)], axis=0)
    prod_after, local_part = lax.associative_scan(compose, (coeff, upstream), reverse=True, axis=0)
    alpha_part = decay_mult[0] * local_part[0]
    beta_part = decay_mult[0] * prod_after[0]
    carried = prefix(
        (beta_part, alpha_part),
        "sp",
        chain_join,
        (jnp.ones_like(beta_part), jnp.zeros_like(alpha_part)),
    )
    incoming = carried[1]
    dstate = local_part + prod_after * incoming[None, :]
    scale_slope = jnp.where(spare_room > 0.01, -decay_mult * decay_mult / in_scale, 0.0)
    log_grad = dstate * (
        memory_hidden_values.astype(jnp.float32) - drive + scale_slope * inp_open * xin
    )
    grad_rec = (
        log_grad
        * (-8.0 * feature_fading_speed[None, :])
        * memory_switch_fraction
        * (1.0 - memory_switch_fraction)
    ).astype(jnp.bfloat16)
    grad_in = (dstate * in_scale * xin * inp_open * (1.0 - inp_open)).astype(jnp.bfloat16)
    back_rec = jnp.einsum(
        "tnd,ncd->tnc",
        grad_rec.reshape(tok_rows, blocks_here, block_width),
        memory_switch_tiles,
        preferred_element_type=jnp.float32,
    )
    back_in = jnp.einsum(
        "tnd,ncd->tnc",
        grad_in.reshape(tok_rows, blocks_here, block_width),
        entry_switch_tiles,
        preferred_element_type=jnp.float32,
    )
    lru_input_grad = (
        dstate * in_scale * inp_open
        + back_rec.reshape(tok_rows, col_count)
        + back_in.reshape(tok_rows, col_count)
    )
    columns = mixed_grad
    out_proj_grad = lax.psum_scatter(
        jnp.einsum("tr,tc->rc", columns, memory_hidden_values, preferred_element_type=jnp.float32),
        "sp",
        scatter_dimension=0,
        tiled=True,
    )
    return (
        gate_weight_grad[None],
        up_weight_grad[None],
        down_grad[None],
        out_proj_grad,
        lru_input_grad,
    )


def direct(
    result_cotangent_values,
    specialist_entry_vectors,
    chosen_specialists,
    specialist_mixing_shares,
    specialist_switch_maps,
    specialist_widen_maps,
    specialist_shrink_maps,
    memory_readout_map,
    memory_source_vectors,
    memory_hidden_values,
    feature_fading_speed,
    extra_log_fading,
    memory_switch_tiles,
    entry_switch_tiles,
):
    tok_rows, feature_count = result_cotangent_values.shape
    sp_count = lax.axis_size("sp")
    info = jnp.concatenate(
        [
            chosen_specialists.astype(jnp.float32).T,
            specialist_mixing_shares.T,
            jnp.zeros((4, tok_rows), jnp.float32),
        ],
        axis=0,
    )
    inputs, all_grad, info, readout, hidden_all = gather_all(
        sp_count,
        specialist_entry_vectors,
        result_cotangent_values,
        info,
        memory_readout_map,
        memory_hidden_values,
    )
    expert = (lax.axis_index("sp") // SLICES).astype(jnp.float32)
    info = info.reshape(sp_count, 8, tok_rows)
    share = jnp.where(info[:, 0] == expert, info[:, 2], 0.0) + jnp.where(
        info[:, 1] == expert, info[:, 3], 0.0
    )
    grads_in = (share.reshape(-1, 1) * all_grad.astype(jnp.float32)).astype(jnp.bfloat16)
    gate_weight_grad, up_weight_grad, down_grad, token_part = expert_backward(
        inputs,
        grads_in,
        specialist_switch_maps[0],
        specialist_widen_maps[0],
        specialist_shrink_maps[0],
    )
    mixed_grad = return_all(
        sp_count, token_part.astype(jnp.bfloat16), result_cotangent_values
    )
    col_count = memory_readout_map.shape[1]
    upstream = jnp.dot(mixed_grad, readout, preferred_element_type=jnp.float32)
    blocks_here = memory_switch_tiles.shape[0]
    block_width = memory_switch_tiles.shape[1]
    blocks_in = memory_source_vectors.reshape(tok_rows, blocks_here, block_width)
    memory_switch_fraction = jax.nn.sigmoid(
        jnp.einsum(
            "tnc,ncd->tnd", blocks_in, memory_switch_tiles, preferred_element_type=jnp.float32
        ).reshape(tok_rows, col_count)
    )
    inp_open = jax.nn.sigmoid(
        jnp.einsum(
            "tnc,ncd->tnd", blocks_in, entry_switch_tiles, preferred_element_type=jnp.float32
        ).reshape(tok_rows, col_count)
    )
    xin = memory_source_vectors.astype(jnp.float32)
    log_fading_factor = (
        -8.0 * memory_switch_fraction * feature_fading_speed[None, :] + extra_log_fading[:, None]
    )
    decay_mult = jnp.exp(log_fading_factor)
    spare_room = -jnp.expm1(2.0 * log_fading_factor)
    in_scale = jnp.sqrt(jnp.maximum(spare_room, 0.01))
    drive = in_scale * inp_open * xin
    dstate, mixed_cols = carry_all(sp_count, mixed_grad, decay_mult, upstream)
    scale_slope = jnp.where(spare_room > 0.01, -decay_mult * decay_mult / in_scale, 0.0)
    log_grad = dstate * (
        memory_hidden_values.astype(jnp.float32) - drive + scale_slope * inp_open * xin
    )
    grad_rec = (
        log_grad
        * (-8.0 * feature_fading_speed[None, :])
        * memory_switch_fraction
        * (1.0 - memory_switch_fraction)
    ).astype(jnp.bfloat16)
    grad_in = (dstate * in_scale * xin * inp_open * (1.0 - inp_open)).astype(jnp.bfloat16)
    back_rec = jnp.einsum(
        "tnd,ncd->tnc",
        grad_rec.reshape(tok_rows, blocks_here, block_width),
        memory_switch_tiles,
        preferred_element_type=jnp.float32,
    )
    back_in = jnp.einsum(
        "tnd,ncd->tnc",
        grad_in.reshape(tok_rows, blocks_here, block_width),
        entry_switch_tiles,
        preferred_element_type=jnp.float32,
    )
    lru_input_grad = (
        dstate * in_scale * inp_open
        + back_rec.reshape(tok_rows, col_count)
        + back_in.reshape(tok_rows, col_count)
    )
    out_proj_grad = jnp.einsum(
        "tr,tc->rc", mixed_cols, hidden_all, preferred_element_type=jnp.float32
    )
    return (
        gate_weight_grad[None],
        up_weight_grad[None],
        down_grad[None],
        out_proj_grad,
        lru_input_grad,
    )


def solution(mesh):
    sp_count, tp_count = mesh.shape["sp"], mesh.shape["tp"]
    whole_blocks = 4 * SLICES == sp_count and tp_count == 4
    return jax.shard_map(
        direct if whole_blocks else local,
        mesh=mesh,
        in_specs=(
            P("sp", None),
            P("sp", None),
            P("sp", None),
            P("sp", None),
            P("sp", None, "tp"),
            P("sp", None, "tp"),
            P("sp", "tp", None),
            P("sp", "tp"),
            P("sp", "tp"),
            P("sp", "tp"),
            P("tp"),
            P("sp"),
            P("tp", None, None),
            P("tp", None, None),
        ),
        out_specs=(
            P("sp", None, "tp"),
            P("sp", None, "tp"),
            P("sp", "tp", None),
            P("sp", "tp"),
            P("sp", "tp"),
        ),
        check_vma=False,
    )
```

profile of v0, /device:TPU:0, one launch (start us, length us, event | category | flops | bytes accessed | tf_op | source)
XLA Modules:
  0.0 202.2 jit_solution(6632460530383640976)
XLA Ops:
  0.6 0.8 convert_bitcast_fusion
  1.5 1.3 maximum_maximum_fusion.info_ref
  2.9 90.4 %shard_map.173 = (bf16[1024,2048]{1,0:T(8,128)(2,1)}, bf16[1024,2048]{1,0:T(8,128)(2,1)}, f32[64,128]{1,0:T(8,128)}, bf16[2048,512]{1,0:T(8,128)(2,1)}, bf16[1024,512]{1,0:T(8,128)(2,1)}) custom-call(bf16[128,2048]{1,0:T(8,128)(2,1)} %x_ref.1, bf16[128,2048]{1,0:T(8,128)(2,1)} %g_ref.3, f32[8,128]{1,0:T(8,128)} %maximum_maximum_fusion.info_ref, ...), custom_call_target="tpu_custom_call" | custom-call | tf_op jit(solution)/shard_map/pallas_call | solution.py:209
  93.4 5.7 %fusion.5 = f32[1024,448]{0,1:T(8,128)} fusion(bf16[1024,2048]{1,0:T(8,128)(2,1)} %get-tuple-element.12, bf16[1,2048,448]{1,2,0:T(8,128)(2,1)S(1)} %copy-done), kind=kOutput, calls=%fused_computation.10 | convolution fusion | flops 1879048192 | bytes 7864320 | tf_op jit(solution)/shard_map/dot_general | solution.py:43
  99.0 3.3 %fusion.8 = f32[1024,448]{0,1:T(8,128)} fusion(bf16[1024,2048]{1,0:T(8,128)(2,1)S(1)} %copy-done.12, bf16[1,2048,448]{1,2,0:T(8,128)(2,1)S(1)} %copy-done.14), kind=kOutput, calls=%fused_computation.13 | convolution fusion | flops 1879048192 | bytes 7864320 | tf_op jit(solution)/shard_map/dot_general | solution.py:44
  102.4 6.6 %multiply_convert_fusion.2 = (bf16[1024,448]{0,1:T(8,128)(2,1)S(1)}, bf16[1024,448]{0,1:T(8,128)(2,1)S(1)}) fusion(f32[1024,448]{0,1:T(8,128)} %fusion.5, f32[1024,448]{0,1:T(8,128)} %fusion.8, bf16[1,448,2048]{2,1,0:T(8,128)(2,1)} %param.20, bf16[1024,2048]{1,0:T(8,128)(2,1)} %get-tuple-element.14, f32[1024]{0:T(1024)S(1)} %bitcast.79), kind=kOutput, calls=%fused_computation.18 | convolution fusion | flops 1891303424 | bytes 11538432 | tf_op jit(solution)/shard_map/rd,fd->rf/dot_general | solution.py:50
  109.1 3.3 %fusion.1 = bf16[1,2048,448]{1,2,0:T(8,128)(2,1)} fusion(bf16[1024,448]{0,1:T(8,128)(2,1)S(1)} %get-tuple-element.20, bf16[1024,2048]{1,0:T(8,128)(2,1)S(1)} %copy-done.13), kind=kOutput, calls=%fused_computation.6 | convolution fusion | flops 1879965696 | bytes 6946816 | tf_op jit(solution)/shard_map/rd,rf->df/dot_general | solution.py:53
  112.4 3.3 %fusion.2 = bf16[1,2048,448]{1,2,0:T(8,128)(2,1)} fusion(bf16[1024,448]{0,1:T(8,128)(2,1)S(1)} %get-tuple-element.19, bf16[1024,2048]{1,0:T(8,128)(2,1)S(1)} %copy-done.13), kind=kOutput, calls=%fused_computation.7 | convolution fusion | flops 1879965696 | bytes 6946816 | tf_op jit(solution)/shard_map/rd,rf->df/dot_general | solution.py:56
  115.7 0.4 copy-done.17
  116.2 3.8 %fusion = bf16[1,448,2048]{2,1,0:T(8,128)(2,1)} fusion(bf16[1024,2048]{1,0:T(8,128)(2,1)S(1)} %copy-done.11, f32[1024]{0:T(1024)S(1)} %bitcast.80, f32[1024,448]{0,1:T(8,128)S(1)} %copy-done.17, f32[1024,448]{0,1:T(8,128)S(1)} %copy-done.16), kind=kOutput, calls=%fused_computation.5 | convolution fusion | flops 1889009664 | bytes 9703424 | tf_op jit(solution)/shard_map/rf,rd->fd/dot_general | solution.py:47
  119.9 2.4 %fusion.3 = f32[1024,2048]{1,0:T(8,128)S(1)} fusion(bf16[1024,448]{0,1:T(8,128)(2,1)S(1)} %get-tuple-element.20, bf16[1,2048,448]{1,2,0:T(8,128)(2,1)S(1)} %copy-done), kind=kOutput, calls=%fused_computation.8 | convolution fusion | flops 1879048192 | bytes 11141120 | tf_op jit(solution)/shard_map/rf,df->rd/dot_general | solution.py:59
  122.3 4.5 %add_convert_fusion.p_ref = bf16[1024,2048]{1,0:T(8,128)(2,1)} fusion(f32[1024,2048]{1,0:T(8,128)S(1)} %fusion.3, bf16[1024,448]{0,1:T(8,128)(2,1)S(1)} %get-tuple-element.19, bf16[1,2048,448]{1,2,0:T(8,128)(2,1)S(1)} %copy-done.15), kind=kOutput, calls=%fused_computation | convolution fusion | flops 1883242496 | bytes 15335424 | tf_op jit(solution)/shard_map/rf,df->rd/dot_general | solution.py:60
  126.9 44.2 %shard_map.174.mixed = bf16[128,2048]{1,0:T(8,128)(2,1)} custom-call(bf16[1024,2048]{1,0:T(8,128)(2,1)} %add_convert_fusion.p_ref, bf16[128,2048]{1,0:T(8,128)(2,1)} %g_ref.3), custom_call_target="tpu_custom_call" | custom-call | tf_op jit(solution)/shard_map/pallas_call | solution.py:274
  171.2 0.3 fusion.18
  171.6 0.2 copy-done.10
  171.8 0.8 fusion.33.decay_ref
  172.6 2.7 %fusion.45.up_ref = f32[128,512]{1,0:T(8,128)} fusion(bf16[128,2048]{1,0:T(8,128)(2,1)S(1)} %copy-done.1, bf16[2048,512]{1,0:T(8,128)(2,1)} %get-tuple-element.15), kind=kOutput, calls=%fused_computation.70 | convolution fusion | flops 268435456 | bytes 2883584 | tf_op jit(solution)/shard_map/dot_general | solution.py:573
  175.4 20.8 %shard_map.175 = (f32[128,512]{1,0:T(8,128)}, bf16[1024,256]{1,0:T(8,128)(2,1)}) custom-call(bf16[128,2048]{1,0:T(8,128)(2,1)} %shard_map.174.mixed, f32[128,512]{1,0:T(8,128)} %fusion.33.decay_ref, f32[128,512]{1,0:T(8,128)} %fusion.45.up_ref), custom_call_target="tpu_custom_call" | custom-call | tf_op jit(solution)/shard_map/pallas_call | solution.py:337
  196.2 2.7 %fusion.46 = f32[256,512]{1,0:T(8,128)} fusion(bf16[1024,256]{1,0:T(8,128)(2,1)} %get-tuple-element.16, bf16[1024,512]{1,0:T(8,128)(2,1)} %get-tuple-element.17), kind=kOutput, calls=%fused_computation.71 | convolution fusion | flops 268435456 | bytes 2097152 | tf_op jit(solution)/shard_map/tr,tc->rc/dot_general | solution.py:624
  198.9 0.3 fusion.15
  199.3 1.4 fusion.26
  200.7 0.2 convolution_bitcast_fusion
  201.0 0.2 convolution_bitcast_fusion.1
  201.2 1.0 add_add_fusion
  (42 shorter events, 0.5 us)
Async XLA Ops:
  0.6 92.7 %copy-start = (bf16[1,2048,448]{1,2,0:T(8,128)(2,1)S(1)}, bf16[1,2048,448]{1,2,0:T(8,128)(2,1)}, u32[]{:S(2)}) copy-start(bf16[1,2048,448]{1,2,0:T(8,128)(2,1)} %param.18) | copy-start | bytes 5505028
  93.3 5.7 %copy-start.12 = (bf16[1024,2048]{1,0:T(8,128)(2,1)S(1)}, bf16[1024,2048]{1,0:T(8,128)(2,1)}, u32[]{:S(2)}) copy-start(bf16[1024,2048]{1,0:T(8,128)(2,1)} %get-tuple-element.12) | copy-start | bytes 12582916
  93.3 5.7 %copy-start.14 = (bf16[1,2048,448]{1,2,0:T(8,128)(2,1)S(1)}, bf16[1,2048,448]{1,2,0:T(8,128)(2,1)}, u32[]{:S(2)}) copy-start(bf16[1,2048,448]{1,2,0:T(8,128)(2,1)} %param.19) | copy-start | bytes 5505028
  99.0 3.3 %copy-start.8 = (f32[64,128]{1,0:T(8,128)S(1)}, f32[64,128]{1,0:T(8,128)}, u32[]{:S(2)}) copy-start(f32[64,128]{1,0:T(8,128)} %get-tuple-element.13) | copy-start | bytes 98308
  102.4 6.7 %copy-start.13 = (bf16[1024,2048]{1,0:T(8,128)(2,1)S(1)}, bf16[1024,2048]{1,0:T(8,128)(2,1)}, u32[]{:S(2)}) copy-start(bf16[1024,2048]{1,0:T(8,128)(2,1)} %get-tuple-element.12) | copy-start | bytes 12582916
  112.4 3.3 %copy-start.11 = (bf16[1024,2048]{1,0:T(8,128)(2,1)S(1)}, bf16[1024,2048]{1,0:T(8,128)(2,1)}, u32[]{:S(2)}) copy-start(bf16[1024,2048]{1,0:T(8,128)(2,1)} %get-tuple-element.14) | copy-start | bytes 12582916
  112.4 3.3 %copy-start.16 = (f32[1024,448]{0,1:T(8,128)S(1)}, f32[1024,448]{0,1:T(8,128)}, u32[]{:S(2)}) copy-start(f32[1024,448]{0,1:T(8,128)} %fusion.5) | copy-start | bytes 5505028
  112.4 3.8 %copy-start.17 = (f32[1024,448]{0,1:T(8,128)S(1)}, f32[1024,448]{0,1:T(8,128)}, u32[]{:S(2)}) copy-start(f32[1024,448]{0,1:T(8,128)} %fusion.8) | copy-start | bytes 5505028
  119.9 2.4 %copy-start.15 = (bf16[1,2048,448]{1,2,0:T(8,128)(2,1)S(1)}, bf16[1,2048,448]{1,2,0:T(8,128)(2,1)}, u32[]{:S(2)}) copy-start(bf16[1,2048,448]{1,2,0:T(8,128)(2,1)} %param.19) | copy-start | bytes 5505028
  126.9 44.2 %copy-start.5 = (bf16[2,256,256]{2,1,0:T(8,128)(2,1)S(1)}, bf16[2,256,256]{2,1,0:T(8,128)(2,1)}, u32[]{:S(2)}) copy-start(bf16[2,256,256]{2,1,0:T(8,128)(2,1)} %param.26) | copy-start | bytes 786436
  126.9 44.3 %copy-start.6 = (bf16[128,512]{1,0:T(8,128)(2,1)S(1)}, bf16[128,512]{1,0:T(8,128)(2,1)}, u32[]{:S(2)}) copy-start(bf16[128,512]{1,0:T(8,128)(2,1)} %param.22) | copy-start | bytes 393220
  171.1 0.7 copy-start.10
  171.1 0.7 copy-start.9
  171.1 1.5 copy-start.1
  175.3 23.5 %copy-start.4 = (bf16[2,256,256]{2,1,0:T(8,128)(2,1)S(1)}, bf16[2,256,256]{2,1,0:T(8,128)(2,1)}, u32[]{:S(2)}) copy-start(bf16[2,256,256]{2,1,0:T(8,128)(2,1)} %param.27) | copy-start | bytes 786436
  175.4 23.5 %copy-start.7 = (bf16[128,512]{1,0:T(8,128)(2,1)S(1)}, bf16[128,512]{1,0:T(8,128)(2,1)}, u32[]{:S(2)}) copy-start(bf16[128,512]{1,0:T(8,128)(2,1)} %param.22) | copy-start | bytes 393220
  196.2 3.1 %copy-start.2 = (f32[128,512]{1,0:T(8,128)S(1)}, f32[128,512]{1,0:T(8,128)}, u32[]{:S(2)}) copy-start(f32[128,512]{1,0:T(8,128)} %get-tuple-element.18) | copy-start | bytes 786436
  196.2 3.1 %copy-start.3 = (bf16[128,512]{1,0:T(8,128)(2,1)S(1)}, bf16[128,512]{1,0:T(8,128)(2,1)}, u32[]{:S(2)}) copy-start(bf16[128,512]{1,0:T(8,128)(2,1)} %h_ref.1) | copy-start | bytes 393220
where the time goes:
time: 203 us; the launch traced here: 202 us
  Pallas kernels  155 us (76%)
  matrix products  39.5 us (19%)
  other arithmetic  5.37 us (3%)
    pallas_call x1, Pallas kernels, gather_all(): pl.pallas_call(functools.partial(gather_kernel, sp_count), out_shape=outs...  90.4 us
    pallas_call x1, Pallas kernels, return_all(): pl.pallas_call(functools.partial(return_kernel, sp_count), out_shape=jax....  44.2 us
    pallas_call x1, Pallas kernels, carry_all(): pl.pallas_call(functools.partial(carry_kernel, sp_count), out_shape=[jax....  20.8 us
    dot_general x1, matrix products, expert_backward(): jnp.einsum('rd,fd->rf', grads_in, down_weight, preferred_element_type=jnp...  6.64 us
    dot_general x1, matrix products, expert_backward(): jnp.dot(inputs, gate_weight, preferred_element_type=jnp.float32)  5.66 us
    dot_general x1, matrix products, expert_backward(): jnp.einsum('rf,df->rd', up_grad, up_weight, preferred_element_type=jnp.fl...  4.54 us

commit v1 on v0

v1 whole, which is shorter than its diff:
```python
import functools

import jax
import jax.numpy as jnp
from jax import lax
from jax.experimental import pallas as pl
from jax.experimental.pallas import tpu as pltpu
from jax.sharding import PartitionSpec as P

SLICES = 2


def prefix(part, axis, combine, identity):
    count = lax.axis_size(axis)
    place = lax.axis_index(axis)
    ahead = count - 1 - place
    gathered = jax.tree.map(lambda a: lax.all_gather(a, axis), part)
    state = jax.tree.map(lambda a, e: jnp.zeros_like(a) + jnp.asarray(e, a.dtype), part, identity)

    def one(turn, state):
        source = count - 1 - turn
        return combine(
            state, jax.tree.map(lambda a: lax.dynamic_index_in_dim(a, source, 0, False), gathered)
        )

    return lax.fori_loop(0, ahead, one, state)


def silu_slope(value):
    sig_value = jax.nn.sigmoid(value)
    return sig_value * (1.0 + value * (1.0 - sig_value))


def compose(upper_map, lower_map):
    return (lower_map[0] * upper_map[0], lower_map[1] + lower_map[0] * upper_map[1])


def chain_join(higher_map, lower_map):
    return (lower_map[0] * higher_map[0], lower_map[1] + lower_map[0] * higher_map[1])


def expert_backward(inputs, grads_in, gate_weight, up_weight, down_weight):
    gate_value = jnp.dot(inputs, gate_weight, preferred_element_type=jnp.float32)
    up_value = jnp.dot(inputs, up_weight, preferred_element_type=jnp.float32)
    active = jax.nn.silu(gate_value)
    hidden = (active * up_value).astype(jnp.bfloat16)
    down_grad = jnp.einsum(
        "rf,rd->fd", hidden, grads_in, preferred_element_type=jnp.float32
    ).astype(jnp.bfloat16)
    hidden_grad = jnp.einsum("rd,fd->rf", grads_in, down_weight, preferred_element_type=jnp.float32)
    gate_grad = (hidden_grad * up_value * silu_slope(gate_value)).astype(jnp.bfloat16)
    up_grad = (hidden_grad * active).astype(jnp.bfloat16)
    gate_weight_grad = jnp.einsum(
        "rd,rf->df", inputs, gate_grad, preferred_element_type=jnp.float32
    ).astype(jnp.bfloat16)
    up_weight_grad = jnp.einsum(
        "rd,rf->df", inputs, up_grad, preferred_element_type=jnp.float32
    ).astype(jnp.bfloat16)
    token_part = jnp.einsum("rf,df->rd", gate_grad, gate_weight, preferred_element_type=jnp.float32)
    token_part = token_part + jnp.einsum(
        "rf,df->rd", up_grad, up_weight, preferred_element_type=jnp.float32
    )
    return (gate_weight_grad, up_weight_grad, down_grad, token_part)


def collect(returned, targets, route_count):
    gathered = jnp.take(returned, targets[0], axis=0).astype(jnp.float32)
    for target in targets[1:]:
        gathered = gathered + jnp.take(returned, target, axis=0).astype(jnp.float32)
    return gathered.reshape(-1, route_count, gathered.shape[-1]).sum(axis=1)


def fill_slots(values, targets, slot_rows):
    buffer = jnp.zeros((slot_rows, values.shape[1]), jnp.bfloat16)
    for target in targets:
        buffer = buffer.at[target].set(values)
    return buffer


MESH_ID = pl.DeviceIdType.MESH


def greet(peers):
    barrier = pltpu.get_barrier_semaphore()
    for peer in peers:
        pl.semaphore_signal(barrier, inc=1, device_id=peer, device_id_type=MESH_ID)
    pl.semaphore_wait(barrier, len(peers))


def remote(src, dst, send, recv, peer):
    return pltpu.make_async_remote_copy(
        src_ref=src, dst_ref=dst, send_sem=send, recv_sem=recv, device_id=peer, device_id_type=MESH_ID
    )


def places(sp_count):
    me = lax.axis_index("sp")
    tp = lax.axis_index("tp")
    side, core = tp // 2, tp % 2
    peers = [(lax.rem(me + k, sp_count), tp) for k in range(sp_count)]
    sources = [lax.rem(me + sp_count - k, sp_count) for k in range(sp_count)]
    sibling = (me, side * 2 + (1 - core))
    across = (me, (1 - side) * 2 + core)
    return me, side, core, peers, sources, sibling, across


NN = (((1,), (0,)), ((), ()))
NT = (((1,), (1,)), ((), ()))
TN = (((0,), (0,)), ((), ()))


def mm(a, b, dims):
    return lax.dot_general(a, b, dims, preferred_element_type=jnp.float32)


def f32(a):
    return a.astype(jnp.float32)


def b16(a):
    return a.astype(jnp.bfloat16)


def mega_kernel(
    sp_count,
    x_ref, g_ref, ch_ref, mix_ref, r_ref, src_ref, h_ref, fade_ref, extra_ref, mt_ref, et_ref,
    wg_any, wu_any, wd_any,
    gw_any, uw_any, dw_any, outp_ref, lru_ref,
    X, Y, sbuf, wg, wu, wd, hid, dg, du, pa, sib, s1, ygot, s2, xgot, s3, s30, zgot,
    gx, M4, Rd, H, MC, gwv, uwv, dwv, ubuf, ugot, Uf, coef, pm, blk, got,
    ssem, rsem, lsem,
):
    me, side, core, peers, sources, sibling, across = places(sp_count)
    tp = lax.axis_index("tp")
    rows, feats = x_ref.shape
    half, quarter, eighth = feats // 2, feats // 4, feats // 8
    passed = 3 * half // 8
    direct = half - passed
    depth = sp_count // 2
    pair = 2 * rows
    z, x = me // 2, me % 2
    partner = (z * 2 + 1 - x, tp)
    plane = [lax.rem(z + k, depth) for k in range(depth)]
    line = [lax.rem(z + depth - k, depth) for k in range(depth)]
    along = [(plane[k] * 2 + x, tp) for k in range(depth)]
    behind = [(line[k] * 2 + x, tp) for k in range(depth)]
    first = pl.multiple_of(core * half + side * passed, 128)
    onward = pl.multiple_of(core * half + side * direct, 128)
    back = pl.multiple_of(core * half + (1 - side) * direct, 128)
    mine = pl.ds(pl.multiple_of(core * half, half), half)
    theirs = pl.ds(pl.multiple_of((1 - core) * half, half), half)
    own_q = pl.ds(pl.multiple_of(side * quarter, quarter), quarter)
    other_q = pl.ds(pl.multiple_of((1 - side) * quarter, quarter), quarter)
    own_e = pl.ds(pl.multiple_of(x * eighth, eighth), eighth)
    other_e = pl.ds(pl.multiple_of((1 - x) * eighth, eighth), eighth)
    own_rows = pl.ds(pl.multiple_of(x * rows, rows), rows)
    other_rows = pl.ds(pl.multiple_of((1 - x) * rows, rows), rows)
    spot = core * 2 + side
    count = [0]
    waiting = []

    def send(src, dst, peer):
        n = count[0]
        count[0] += 1
        cp = remote(src, dst, ssem.at[n], rsem.at[n], peer)
        cp.start()
        waiting.append(cp)
        return cp

    def at(ref, who, col, width):
        return ref.at[pl.ds(pl.multiple_of(who * rows, rows), rows), pl.ds(col, width)]

    def block(ref, who):
        return pl.ds(pl.multiple_of(who * rows, rows), rows)

    local = []
    for n, (src, dst) in enumerate(((wg_any, wg), (wu_any, wu), (wd_any, wd))):
        cp = pltpu.make_async_copy(src, dst, lsem.at[n])
        cp.start()
        local.append(cp)

    barrier = pltpu.get_barrier_semaphore()
    friends = peers[1:] + [sibling, across]
    for friend in friends:
        pl.semaphore_signal(barrier, inc=1, device_id=friend, device_id_type=MESH_ID)

    chosen, mix = ch_ref[...], mix_ref[...]

    def share(expert):
        return jnp.sum(jnp.where(chosen == expert, mix, 0.0), axis=1, keepdims=True)

    here_rows = block(X, me)
    X[here_rows, :] = x_ref[...]
    Y[here_rows, :] = b16(share(z) * f32(g_ref[...]))
    for k in range(1, depth):
        sbuf[k - 1] = b16(share(plane[k]) * f32(g_ref[:, pl.ds(first, direct)]))
    Rd[z] = r_ref[...]
    H[here_rows, :] = h_ref[...]
    pl.semaphore_wait(barrier, len(friends))

    zc, xc, yc, sc, tc = {}, {}, {}, {}, {}
    bufs = (X, Y)

    def send_z(a, k):
        src = x_ref.at[:, pl.ds(first, direct)] if a == 0 else sbuf.at[k - 1]
        zc[a, k] = send(src, at(bufs[a], me, first, direct), along[k])

    def send_x(a, k, who):
        src = x_ref.at[:, pl.ds(first, direct)] if (a == 0 and k == 0) else at(bufs[a], who, first, direct)
        xc[a, k] = send(src, at(bufs[a], who, first, direct), partner)

    def spread(a, who, n):
        ref = bufs[a]
        yc[a, n] = send(at(ref, who, onward, passed), at(ref, who, onward, passed), across)
        sc[a, n] = send(at(ref, who, first, direct), at(ref, who, first, direct), sibling)

    def source(n):
        return line[n] * 2 + x if n < depth else line[n - depth] * 2 + 1 - x

    def event_z(k):
        for a in range(2):
            zc[a, k].wait_recv()
            send_x(a, k, source(k))
            spread(a, source(k), k)

    def event_x(k):
        for a in range(2):
            xc[a, k].wait_recv()
            spread(a, source(depth + k), depth + k)

    def event_y(*ns):
        for n in ns:
            for a in range(2):
                yc[a, n].wait_recv()
                tc[a, n] = send(at(bufs[a], source(n), back, passed), at(bufs[a], source(n), back, passed), sibling)

    def settle(*ns):
        for n in ns:
            for a in range(2):
                sc[a, n].wait_recv()
                tc[a, n].wait_recv()

    def stage_a(k):
        at_rows = pl.ds(pl.multiple_of(line[k] * pair, pair), pair)
        xv = X[at_rows, :]
        gate = mm(xv, wg[...], NT)
        up = mm(xv, wu[...], NT)
        back_value = mm(Y[at_rows, :], wd[...], NT)
        sig = jax.nn.sigmoid(gate)
        act = gate * sig
        hid[at_rows, :] = b16(act * up)
        dg[at_rows, :] = b16(back_value * up * (sig * (1.0 + gate * (1.0 - sig))))
        du[at_rows, :] = b16(back_value * act)

    r1, r2, r3, r4 = {}, {}, {}, {}

    def stage_b(k):
        at_rows = pl.ds(pl.multiple_of(line[k] * pair, pair), pair)
        dgv, duv = dg[at_rows, :], du[at_rows, :]
        for cols in (theirs, mine):
            pa[k, :, cols] = b16(mm(dgv, wg[:, cols], NN) + mm(duv, wu[:, cols], NN))
            if cols is theirs:
                r1[k] = send(pa.at[k, :, theirs], sib.at[k], sibling)

    def fold_core(k):
        r1[k].wait_recv()
        s1[k] = b16(f32(pa[k, :, mine]) + f32(sib[k]))
        r2[k] = send(s1.at[k, :, other_q], ygot.at[k], across)

    def fold_y(k):
        r2[k].wait_recv()
        s2[k] = b16(f32(s1[k, :, own_q]) + f32(ygot[k]))
        r3[k] = send(s2.at[k, :, other_e], xgot.at[k], partner)

    def fold_x(k):
        r3[k].wait_recv()
        total = f32(s2[k, :, own_e]) + f32(xgot[k])
        if k == 0:
            s30[...] = total
        else:
            s3[k] = b16(total)
            r4[k] = send(s3.at[k], zgot.at[k], behind[k])

    tile = quarter
    grads = ((dg, X, gwv, gw_any), (du, X, uwv, uw_any), (hid, Y, dwv, dw_any))

    def weight_grad(n, *tiles):
        lhs, rhs, dst, out = grads[n]
        for i in tiles:
            dst[:, i * tile:(i + 1) * tile] = b16(mm(lhs[...], rhs[:, i * tile:(i + 1) * tile], TN))
            if (i + 1) * tile == feats:
                cp = pltpu.make_async_copy(dst, out, lsem.at[3 + n])
                cp.start()
                local.append(cp)

    for k in range(1, depth):
        send_z(0, k)
        if k == 1:
            send_x(0, 0, me)
        send_z(1, k)
        if k == 1:
            send_x(1, 0, me)

    blocks = mt_ref.shape[0]
    width = mt_ref.shape[1]
    source_value = src_ref[...]
    rec = jnp.concatenate(
        [mm(source_value[:, n * width:(n + 1) * width], mt_ref[n], NN) for n in range(blocks)], axis=1
    )
    inp = jnp.concatenate(
        [mm(source_value[:, n * width:(n + 1) * width], et_ref[n], NN) for n in range(blocks)], axis=1
    )
    rec, inp = jax.nn.sigmoid(rec), jax.nn.sigmoid(inp)
    xin = f32(source_value)
    rate = -8.0 * fade_ref[...]
    log_decay = rec * rate + extra_ref[...]
    decay = jnp.exp(log_decay)
    spare = 1.0 - jnp.exp(2.0 * log_decay)
    in_scale = jnp.sqrt(jnp.maximum(spare, 0.01))
    slope = jnp.where(spare > 0.01, -decay * decay / in_scale, 0.0)
    c4 = in_scale * inp
    coef[0] = (f32(h_ref[...]) - c4 * xin + slope * inp * xin) * rate * rec * (1.0 - rec)
    coef[1] = in_scale * xin * inp * (1.0 - inp)
    coef[2] = c4
    coef[3] = decay
    row = lax.broadcasted_iota(jnp.int32, decay.shape, 0)
    prod = jnp.where(row < rows - 1, pltpu.roll(decay, rows - 1, 0), 1.0)
    step, level = 1, 0
    while step < rows:
        keep = row < rows - step
        pm[level] = jnp.where(keep, prod, 0.0)
        prod = prod * jnp.where(keep, pltpu.roll(prod, rows - step, 0), 1.0)
        step, level = step * 2, level + 1
    coef[4] = prod

    for cp in local[:3]:
        cp.wait()
    event_x(0)
    event_z(1)
    event_y(depth)
    settle(depth)
    stage_a(0)
    event_x(1)
    stage_b(0)
    event_y(1, depth + 1)
    event_z(2)
    settle(1, depth + 1)
    stage_a(1)
    fold_core(0)
    event_x(2)
    stage_b(1)
    event_y(2, depth + 2)
    event_z(3)
    readout = {k: send(r_ref, Rd.at[z], along[k]) for k in range(1, depth)}
    piece = pl.ds(pl.multiple_of(core * half + side * quarter + (1 - x) * eighth, eighth), eighth)
    raw = send(g_ref.at[:, piece], gx, partner)
    settle(2, depth + 2)
    stage_a(2)
    fold_core(1)
    event_x(3)
    stage_b(2)
    fold_y(0)
    event_y(3, depth + 3)
    settle(3, depth + 3)
    stage_a(3)
    fold_core(2)
    stage_b(3)
    fold_y(1)
    fold_x(0)
    fold_core(3)
    weight_grad(0, 0, 1)
    fold_y(2)
    fold_x(1)
    weight_grad(0, 2, 3)
    weight_grad(1, 0)
    fold_y(3)
    fold_x(2)
    weight_grad(1, 1, 2, 3)
    fold_x(3)
    saved = {k: send(h_ref, H.at[here_rows, :], along[k]) for k in range(1, depth)}
    saved_x = {0: send(h_ref, H.at[here_rows, :], partner)}
    weight_grad(2, 0, 1, 2, 3)
    raw.wait_recv()
    for k in range(1, depth):
        r4[k].wait_recv()
    cols = pl.ds(pl.multiple_of(core * half + side * quarter + x * eighth, eighth), eighth)
    for at_rows, value in ((own_rows, g_ref[:, cols]), (other_rows, gx[...])):
        total = s30[at_rows, :]
        for k in range(1, depth):
            total = total + f32(zgot[k, at_rows, :])
        M4[spot, at_rows, :] = b16(f32(value) + total)
    near = send(M4.at[spot], M4.at[spot], across)
    send_s = send(M4.at[spot], M4.at[spot], sibling)
    near.wait_recv()
    spot_y = core * 2 + 1 - side
    send_t = send(M4.at[spot_y], M4.at[spot_y], sibling)
    for k in range(1, depth):
        readout[k].wait_recv()
    send_s.wait_recv()
    send_t.wait_recv()

    def upstream(at_rows):
        return sum(mm(M4[n, at_rows, :], Rd[n], NN) for n in range(depth))

    ubuf[...] = b16(upstream(other_rows))
    cross = send(ubuf, ugot, partner)
    Uf[...] = upstream(own_rows)
    core_rows = pl.ds(pl.multiple_of(core * rows, rows), rows)

    def cell(who):
        return pl.ds(pl.multiple_of(who * pair + core * rows, rows), rows)

    moved = {k: send(M4.at[plane[k], core_rows, :], MC.at[cell(z), :], along[k]) for k in range(1, depth)}
    MC[pl.ds(pl.multiple_of(z * pair, pair), pair), :] = M4[z]
    cross.wait_recv()
    part = Uf[...] + f32(ugot[...])
    step, level = 1, 0
    while step < rows:
        part = part + pm[level] * pltpu.roll(part, rows - step, 0)
        step, level = step * 2, level + 1
    blk[0:1] = coef[3, 0:1] * coef[4, 0:1]
    blk[1:2] = coef[3, 0:1] * part[0:1]
    Uf[...] = part
    carried = {k: send(blk, got.at[me], peers[k]) for k in range(1, sp_count)}
    for k in range(1, depth):
        saved[k].wait_recv()
        at_rows = block(H, source(k))
        saved_x[k] = send(H.at[at_rows, :], H.at[at_rows, :], partner)
    spread_c = {}
    for k in range(1, depth):
        moved[k].wait_recv()
        spread_c[k] = send(MC.at[cell(line[k]), :], MC.at[cell(line[k]), :], sibling)
    for k in range(1, sp_count):
        carried[k].wait_recv()
    incoming = jnp.zeros((1, part.shape[1]), jnp.float32)
    for origin in range(sp_count - 1, 0, -1):
        value = got[origin]
        incoming = jnp.where(origin > me, value[1:2] + value[0:1] * incoming, incoming)
    dstate = Uf[...] + coef[4] * incoming
    grad_rec = b16(dstate * coef[0])
    grad_in = b16(dstate * coef[1])
    back_value = jnp.concatenate(
        [
            mm(grad_rec[:, n * width:(n + 1) * width], mt_ref[n], NT)
            + mm(grad_in[:, n * width:(n + 1) * width], et_ref[n], NT)
            for n in range(blocks)
        ],
        axis=1,
    )
    lru_ref[...] = dstate * coef[2] + back_value
    for k in range(depth):
        saved_x[k].wait_recv()
    for k in range(1, depth):
        spread_c[k].wait_recv()
    outp_ref[...] = mm(MC[...], H[...], TN)
    for cp in waiting:
        cp.wait_send()
    for cp in local[3:]:
        cp.wait()


def mega(sp_count, x, g, chosen, mix, readout, source, hidden, fade, extra, rec_tiles, in_tiles, wg, wu, wd):
    rows, feats = x.shape
    units = wg.shape[0]
    cols = readout.shape[1]
    depth = sp_count // 2
    total, pair, half, quarter, eighth = rows * sp_count, 2 * rows, feats // 2, feats // 4, feats // 8
    direct = half - 3 * half // 8
    levels = (rows - 1).bit_length()
    dma = pltpu.SemaphoreType.DMA

    def vb(*shape):
        return pltpu.VMEM(shape, jnp.bfloat16)

    def vf(*shape):
        return pltpu.VMEM(shape, jnp.float32)

    scratch = [
        vb(total, feats), vb(total, feats), vb(depth - 1, rows, direct),
        vb(units, feats), vb(units, feats), vb(units, feats),
        vb(total, units), vb(total, units), vb(total, units),
        vb(depth, pair, feats), vb(depth, pair, half), vb(depth, pair, half),
        vb(depth, pair, quarter), vb(depth, pair, quarter),
        vb(depth, pair, eighth), vb(depth, pair, eighth), vf(pair, eighth), vb(depth, pair, eighth),
        vb(rows, eighth), vb(depth, pair, eighth), vb(depth, readout.shape[0], cols),
        vb(total, cols), vb(total, eighth),
        vb(units, feats), vb(units, feats), vb(units, feats),
        vb(rows, cols), vb(rows, cols), vf(rows, cols), vf(5, rows, cols), vf(levels, rows, cols),
        vf(8, cols), vf(sp_count, 8, cols),
        dma((128,)), dma((128,)), dma((6,)),
    ]
    vmem, anywhere = pl.BlockSpec(memory_space=pltpu.VMEM), pl.BlockSpec(memory_space=pl.ANY)
    weight = jax.ShapeDtypeStruct((units, feats), jnp.bfloat16)
    return pl.pallas_call(
        functools.partial(mega_kernel, sp_count),
        out_shape=[
            weight, weight, weight,
            jax.ShapeDtypeStruct((eighth, cols), jnp.float32),
            jax.ShapeDtypeStruct((rows, cols), jnp.float32),
        ],
        in_specs=[vmem] * 11 + [anywhere] * 3,
        out_specs=[anywhere] * 3 + [vmem] * 2,
        scratch_shapes=scratch,
        compiler_params=pltpu.CompilerParams(
            collective_id=0, has_side_effects=True, vmem_limit_bytes=58 * 2 ** 20
        ),
    )(x, g, chosen, mix, readout, source, hidden, fade, extra, rec_tiles, in_tiles, wg, wu, wd)


def local(
    result_cotangent_values,
    specialist_entry_vectors,
    chosen_specialists,
    specialist_mixing_shares,
    specialist_switch_maps,
    specialist_widen_maps,
    specialist_shrink_maps,
    memory_readout_map,
    memory_source_vectors,
    memory_hidden_values,
    feature_fading_speed,
    extra_log_fading,
    memory_switch_tiles,
    entry_switch_tiles,
):
    tok_rows, feature_count = result_cotangent_values.shape
    route_count = chosen_specialists.shape[1]
    sp_count = lax.axis_size("sp")
    expert_count = sp_count // SLICES
    capacity = min(tok_rows, 4 * tok_rows // expert_count)
    slot_rows = sp_count * capacity
    flat_expert = chosen_specialists.reshape(-1)
    onehot = (flat_expert[:, None] == jnp.arange(expert_count, dtype=jnp.int32)[None, :]).astype(
        jnp.int32
    )
    slot_rank = jnp.sum((jnp.cumsum(onehot, axis=0) - 1) * onehot, axis=1)
    scaled = (
        (
            specialist_mixing_shares[:, :, None]
            * result_cotangent_values[:, None, :].astype(jnp.float32)
        )
        .astype(jnp.bfloat16)
        .reshape(-1, feature_count)
    )
    copies = jnp.broadcast_to(
        specialist_entry_vectors[:, None, :], (tok_rows, route_count, feature_count)
    ).reshape(-1, feature_count)
    targets = [
        (flat_expert * SLICES + slice_index) * capacity + slot_rank for slice_index in range(SLICES)
    ]
    share = feature_count // lax.axis_size("tp")
    first_col = lax.axis_index("tp") * share
    part_grad = lax.dynamic_slice_in_dim(scaled, first_col, share, 1)
    part_rows = lax.dynamic_slice_in_dim(copies, first_col, share, 1)
    send_grad = fill_slots(part_grad, targets, slot_rows)
    send_rows = fill_slots(part_rows, targets, slot_rows)
    got_grad, got_rows = (
        lax.all_to_all(
            send_grad.reshape(sp_count, capacity, share),
            "sp",
            split_axis=0,
            concat_axis=0,
            tiled=True,
        ),
        lax.all_to_all(
            send_rows.reshape(sp_count, capacity, share),
            "sp",
            split_axis=0,
            concat_axis=0,
            tiled=True,
        ),
    )
    recv_grad, recv_rows = (
        lax.all_gather(got_grad, "tp", axis=2, tiled=True),
        lax.all_gather(got_rows, "tp", axis=2, tiled=True),
    )
    inputs = recv_rows.reshape(slot_rows, feature_count)
    grads_in = recv_grad.reshape(slot_rows, feature_count)
    gate_weight_grad, up_weight_grad, down_grad, token_part = expert_backward(
        inputs,
        grads_in,
        specialist_switch_maps[0],
        specialist_widen_maps[0],
        specialist_shrink_maps[0],
    )
    returned = lax.all_to_all(
        token_part.astype(jnp.bfloat16).reshape(sp_count, capacity, feature_count),
        "sp",
        split_axis=0,
        concat_axis=0,
        tiled=True,
    )
    own_sum = collect(returned.reshape(slot_rows, feature_count), targets, route_count)
    moe_grad = lax.psum(own_sum.astype(jnp.bfloat16), "tp").astype(jnp.float32)
    mixed_grad = (result_cotangent_values.astype(jnp.float32) + moe_grad).astype(jnp.bfloat16)
    col_count = memory_readout_map.shape[1]
    columns = mixed_grad
    upstream = jnp.dot(
        columns,
        lax.all_gather(memory_readout_map, "sp", axis=0, tiled=True),
        preferred_element_type=jnp.float32,
    )
    blocks_here = memory_switch_tiles.shape[0]
    block_width = memory_switch_tiles.shape[1]
    blocks_in = memory_source_vectors.reshape(tok_rows, blocks_here, block_width)
    memory_switch_fraction = jax.nn.sigmoid(
        jnp.einsum(
            "tnc,ncd->tnd", blocks_in, memory_switch_tiles, preferred_element_type=jnp.float32
        ).reshape(tok_rows, col_count)
    )
    inp_open = jax.nn.sigmoid(
        jnp.einsum(
            "tnc,ncd->tnd", blocks_in, entry_switch_tiles, preferred_element_type=jnp.float32
        ).reshape(tok_rows, col_count)
    )
    xin = memory_source_vectors.astype(jnp.float32)
    log_fading_factor = (
        -8.0 * memory_switch_fraction * feature_fading_speed[None, :] + extra_log_fading[:, None]
    )
    decay_mult = jnp.exp(log_fading_factor)
    spare_room = -jnp.expm1(2.0 * log_fading_factor)
    in_scale = jnp.sqrt(jnp.maximum(spare_room, 0.01))
    drive = in_scale * inp_open * xin
    coeff = jnp.concatenate([decay_mult[1:], jnp.ones((1, col_count), jnp.float32)], axis=0)
    prod_after, local_part = lax.associative_scan(compose, (coeff, upstream), reverse=True, axis=0)
    alpha_part = decay_mult[0] * local_part[0]
    beta_part = decay_mult[0] * prod_after[0]
    carried = prefix(
        (beta_part, alpha_part),
        "sp",
        chain_join,
        (jnp.ones_like(beta_part), jnp.zeros_like(alpha_part)),
    )
    incoming = carried[1]
    dstate = local_part + prod_after * incoming[None, :]
    scale_slope = jnp.where(spare_room > 0.01, -decay_mult * decay_mult / in_scale, 0.0)
    log_grad = dstate * (
        memory_hidden_values.astype(jnp.float32) - drive + scale_slope * inp_open * xin
    )
    grad_rec = (
        log_grad
        * (-8.0 * feature_fading_speed[None, :])
        * memory_switch_fraction
        * (1.0 - memory_switch_fraction)
    ).astype(jnp.bfloat16)
    grad_in = (dstate * in_scale * xin * inp_open * (1.0 - inp_open)).astype(jnp.bfloat16)
    back_rec = jnp.einsum(
        "tnd,ncd->tnc",
        grad_rec.reshape(tok_rows, blocks_here, block_width),
        memory_switch_tiles,
        preferred_element_type=jnp.float32,
    )
    back_in = jnp.einsum(
        "tnd,ncd->tnc",
        grad_in.reshape(tok_rows, blocks_here, block_width),
        entry_switch_tiles,
        preferred_element_type=jnp.float32,
    )
    lru_input_grad = (
        dstate * in_scale * inp_open
        + back_rec.reshape(tok_rows, col_count)
        + back_in.reshape(tok_rows, col_count)
    )
    columns = mixed_grad
    out_proj_grad = lax.psum_scatter(
        jnp.einsum("tr,tc->rc", columns, memory_hidden_values, preferred_element_type=jnp.float32),
        "sp",
        scatter_dimension=0,
        tiled=True,
    )
    return (
        gate_weight_grad[None],
        up_weight_grad[None],
        down_grad[None],
        out_proj_grad,
        lru_input_grad,
    )


def direct(
    result_cotangent_values,
    specialist_entry_vectors,
    chosen_specialists,
    specialist_mixing_shares,
    specialist_switch_maps,
    specialist_widen_maps,
    specialist_shrink_maps,
    memory_readout_map,
    memory_source_vectors,
    memory_hidden_values,
    feature_fading_speed,
    extra_log_fading,
    memory_switch_tiles,
    entry_switch_tiles,
):
    gate_weight_grad, up_weight_grad, down_grad, out_proj_grad, lru_input_grad = mega(
        lax.axis_size("sp"),
        specialist_entry_vectors,
        result_cotangent_values,
        chosen_specialists,
        specialist_mixing_shares,
        memory_readout_map,
        memory_source_vectors,
        memory_hidden_values,
        feature_fading_speed[None, :],
        extra_log_fading[:, None],
        memory_switch_tiles,
        entry_switch_tiles,
        jnp.swapaxes(specialist_switch_maps[0], 0, 1),
        jnp.swapaxes(specialist_widen_maps[0], 0, 1),
        specialist_shrink_maps[0],
    )
    return (
        jnp.swapaxes(gate_weight_grad, 0, 1)[None],
        jnp.swapaxes(up_weight_grad, 0, 1)[None],
        down_grad[None],
        out_proj_grad,
        lru_input_grad,
    )


def solution(mesh):
    sp_count, tp_count = mesh.shape["sp"], mesh.shape["tp"]
    whole_blocks = 4 * SLICES == sp_count and tp_count == 4
    return jax.shard_map(
        direct if whole_blocks else local,
        mesh=mesh,
        in_specs=(
            P("sp", None),
            P("sp", None),
            P("sp", None),
            P("sp", None),
            P("sp", None, "tp"),
            P("sp", None, "tp"),
            P("sp", "tp", None),
            P("sp", "tp"),
            P("sp", "tp"),
            P("sp", "tp"),
            P("tp"),
            P("sp"),
            P("tp", None, None),
            P("tp", None, None),
        ),
        out_specs=(
            P("sp", None, "tp"),
            P("sp", None, "tp"),
            P("sp", "tp", None),
            P("sp", "tp"),
            P("sp", "tp"),
        ),
        check_vma=False,
    )
```

time: 203 us -> 141 us (0.69)
  matrix products: 39.5 us -> 0 us
  Pallas kernels: 155 us -> 128 us
  local copies, waits for them, and re-layouts: 1.09 us -> 12.3 us
  other arithmetic: 5.37 us -> 0 us
    dot_general x14 -> x0, matrix products: 39.5 us -> none  [the longest x1 6.64 us: expert_backward(): jnp.einsum('rd,fd->rf', grads_in, down_weight, preferred_element_type=jnp...]
    pallas_call x3 -> x1, Pallas kernels: 155 us -> 128 us  [mega(): pl.pallas_call(functools.partial(mega_kernel, sp_count), out_shape=[weigh...]
    unnamed x36 -> x15, local copies, waits for them, and re-layouts: 0.71 us -> 10.9 us
where the time goes in v1:
time: 141 us
  Pallas kernels  128 us (91%)
  local copies, waits for them, and re-layouts  12.3 us (9%)
    pallas_call x1, Pallas kernels, mega(): pl.pallas_call(functools.partial(mega_kernel, sp_count), out_shape=[weigh...  128 us
    unnamed x15, local copies, waits for them, and re-layouts  10.9 us

profile of v1, /device:TPU:0, one launch (start us, length us, event | category | flops | bytes accessed | tf_op | source)
XLA Modules:
  0.0 140.5 jit_solution(2700500631749914927)
XLA Ops:
  0.6 1.4 %copy.19.ch_ref = s32[128,2]{1,0:T(8,128)} copy(s32[128,2]{0,1:T(2,128)} %param.16) | data formatting | bytes 2048 | tf_op args[2]
  2.0 1.4 %copy.20.mix_ref = f32[128,2]{1,0:T(8,128)} copy(f32[128,2]{0,1:T(2,128)} %param.17) | data formatting | bytes 2048 | tf_op args[3]
  3.5 1.4 copy.21.extra_ref
  4.8 127.5 %shard_map.173 = (bf16[448,2048]{1,0:T(8,128)(2,1)}, bf16[448,2048]{1,0:T(8,128)(2,1)}, bf16[448,2048]{1,0:T(8,128)(2,1)}, f32[256,512]{1,0:T(8,128)}, f32[128,512]{1,0:T(8,128)}) custom-call(bf16[128,2048]{1,0:T(8,128)(2,1)} %x_ref.1, bf16[128,2048]{1,0:T(8,128)(2,1)} %g_ref.1, s32[128,2]{1,0:T(8,128)} %copy.19.ch_ref, f32[128,2]{1,0:T(8,128)} %copy.20.mix_ref, ...), custom_call_target="tpu_custom_call" | custom-call | tf_op jit(solution)/shard_map/pallas_call | solution.py:494
  132.4 0.0 copy-start.1
  132.4 3.1 %copy.27 = bf16[1,2048,448]{1,2,0:T(8,128)(2,1)} copy(bf16[1,2048,448]{1,2,0:T(8,128)(2,1)} %bitcast.18) | data formatting | bytes 3670016
  135.5 0.0 copy-done.1
  135.5 0.0 copy-start
  135.5 1.2 copy.28
  136.7 0.9 copy-done
  137.7 0.0 copy-start.2
  137.7 0.0 copy-start.3
  137.7 1.2 copy.29
  138.9 0.1 copy-done.2
  139.0 0.8 copy.30
  139.8 0.0 copy-done.3
  139.8 0.7 copy.31
Async XLA Ops:
  132.4 3.1 %copy-start.1 = (bf16[448,2048]{1,0:T(8,128)(2,1)S(1)}, bf16[448,2048]{1,0:T(8,128)(2,1)}, u32[]{:S(2)}) copy-start(bf16[448,2048]{1,0:T(8,128)(2,1)} %get-tuple-element.11) | copy-start | bytes 5505028
  135.5 2.2 %copy-start = (bf16[448,2048]{1,0:T(8,128)(2,1)S(1)}, bf16[448,2048]{1,0:T(8,128)(2,1)}, u32[]{:S(2)}) copy-start(bf16[448,2048]{1,0:T(8,128)(2,1)} %get-tuple-element.12) | copy-start | bytes 5505028
  137.7 1.4 copy-start.2
  137.7 2.2 %copy-start.3 = (f32[128,512]{1,0:T(8,128)S(1)}, f32[128,512]{1,0:T(8,128)}, u32[]{:S(2)}) copy-start(f32[128,512]{1,0:T(8,128)} %get-tuple-element.24) | copy-start | bytes 786436
